TPU v7x, 32 devices: a whole 2x2x4 slice. The times are simulated.
32 devices in a mesh: sp: 8 (over z, y), tp: 4 (over x, core).
Axes of the slice: x: 2, y: 2, z: 4, core: 2. Of those that a mesh axis runs over, the one named last changes fastest.
Arguments:
- tokens: bfloat16 [2048, 4096], P(('sp', 'tp')), may hold values from -6 to 6, as said below
- query_one: bfloat16 [4096, 1024], P('sp', 'tp'), may hold values from -0.125 to 0.125
- query_two: bfloat16 [4096, 1024], P('sp', 'tp'), may hold values from -0.125 to 0.125
- key_one: bfloat16 [4096, 1024], P('sp', 'tp'), may hold values from -0.125 to 0.125
- key_two: bfloat16 [4096, 1024], P('sp', 'tp'), may hold values from -0.125 to 0.125
- value_weight: bfloat16 [4096, 2048], P('sp', 'tp'), may hold values from -0.09375 to 0.09375
- out_weight: bfloat16 [2048, 4096], P('tp', 'sp'), may hold values from -0.125 to 0.125
- lambdas: float32 [8], P('tp'), may hold values from 0.3 to 0.8
- head_gain: float32 [256], replicated, may hold values from 0.1 to 1.9
Outputs:
- layer_out: bfloat16 [2048, 4096], P(('sp', 'tp'))
Inputs may be any that keep to these rules, and one draw needn't show every extreme that they name: `tokens`: the features' mean changes between 16 equal spans of the sequence.
All inputs are finite; a program needn't handle non-finite values.
Results may differ from a plain program's by a relative error of at most 0.013.
The roundings to bfloat16 on the way count: a program that leaves them out, or rounds other values in their place, can miss the bound.
Values may be sent and summed in bfloat16 or wider, within the bound.
No kernel may reach another device: no remote copies, remote signals or barrier semaphores. Data moves between devices by JAX's collectives and lax.ppermute only.
A program may use at most 128 MiB of HBM per device.

v0:
```python
import jax
import jax.numpy as jnp
from jax import lax
from jax.sharding import PartitionSpec as P

QK = 128
V = 256
ROPE_BASE = 500000.0
EPS_NORM = 0.02


def rotate(values, positions):
    half_dim = values.shape[-1] // 2
    inverse = 1.0 / ROPE_BASE ** (
        jnp.arange(0, 2 * half_dim, 2, dtype=jnp.float32) / (2 * half_dim)
    )
    angles = positions.astype(jnp.float32)[:, None] * inverse[None, :]
    cos_part = jnp.cos(angles)[:, None, :]
    sin_part = jnp.sin(angles)[:, None, :]
    first_half = values[..., :half_dim]
    second_half = values[..., half_dim:]
    return jnp.concatenate(
        [
            first_half * cos_part - second_half * sin_part,
            second_half * cos_part + first_half * sin_part,
        ],
        axis=-1,
    )


def unchanged(carried):
    return carried


def on_device(
    tokens, query_one, query_two, key_one, key_two, value_weight, out_weight, lambdas, head_gain
):
    tp_count = lax.axis_size("tp")
    sp_index = lax.axis_index("sp")
    own_rows = tokens.shape[0]
    local_len = own_rows * tp_count
    half_len = local_len // 2
    heads_here = lambdas.shape[0]
    gathered = lax.all_gather(tokens, "tp", axis=0, tiled=True)
    row_ids = jnp.arange(local_len, dtype=jnp.int32)
    query_pos = sp_index * local_len + row_ids
    pieces = (
        lax.all_gather(query_one, "sp", axis=0, tiled=True),
        lax.all_gather(query_two, "sp", axis=0, tiled=True),
        lax.all_gather(key_one, "sp", axis=0, tiled=True),
        lax.all_gather(key_two, "sp", axis=0, tiled=True),
        lax.all_gather(value_weight, "sp", axis=0, tiled=True),
    )
    projected = tuple(
        (
            jnp.dot(gathered, weight_piece, preferred_element_type=jnp.float32)
            for weight_piece in pieces
        )
    )

    def turned(product):
        return rotate(product.reshape(local_len, heads_here, QK), query_pos).astype(jnp.bfloat16)

    q_one = turned(projected[0])
    q_two = turned(projected[1])
    k_one = turned(projected[2]).reshape(local_len, heads_here * QK)
    k_two = turned(projected[3]).reshape(local_len, heads_here * QK)
    values = projected[4].astype(jnp.bfloat16)
    scale = QK ** (-0.5)
    pieces = (
        lax.all_gather(k_one, "sp", axis=0, tiled=True),
        lax.all_gather(k_two, "sp", axis=0, tiled=True),
        lax.all_gather(values, "sp", axis=0, tiled=True),
    )
    key_count = pieces[0].shape[0]
    global_ids = jnp.arange(key_count, dtype=jnp.int32)
    shard_ids = global_ids // local_len
    within = global_ids % local_len
    key_pos = shard_ids * local_len + within
    key_sets = (
        pieces[0].reshape(key_count, heads_here, QK),
        pieces[1].reshape(key_count, heads_here, QK),
    )
    value_rows = pieces[2].reshape(key_count, heads_here, V)
    row_tops = jnp.full((2, heads_here, local_len), -1e30, jnp.float32)
    totals = jnp.zeros((2, heads_here, local_len), jnp.float32)
    accums = jnp.zeros((2, heads_here, local_len, V), jnp.float32)
    new_parts = []
    for segment in range(2):
        low_row = segment * half_len
        seg_pos = query_pos[low_row : low_row + half_len]
        queries = (q_one[low_row : low_row + half_len], q_two[low_row : low_row + half_len])
        carried = (
            row_tops[:, :, low_row : low_row + half_len],
            totals[:, :, low_row : low_row + half_len],
            accums[:, :, low_row : low_row + half_len],
        )

        def update(carried, queries=queries, seg_pos=seg_pos):
            allowed = key_pos[None, :] <= seg_pos[:, None]
            out_tops, out_totals, out_accums = ([], [], [])
            for map_index in range(2):
                scores = (
                    jnp.einsum(
                        "qhd,khd->hqk",
                        queries[map_index],
                        key_sets[map_index],
                        preferred_element_type=jnp.float32,
                    )
                    * scale
                )
                masked = jnp.where(allowed[None], scores, -1e30)
                old_top = carried[0][map_index]
                new_top = jnp.maximum(old_top, jnp.max(masked, axis=-1))
                exp_weights = jnp.where(allowed[None], jnp.exp(scores - new_top[..., None]), 0.0)
                new_total = jnp.sum(exp_weights, axis=-1)
                new_accum = jnp.einsum(
                    "hqk,khv->hqv",
                    exp_weights.astype(jnp.bfloat16),
                    value_rows,
                    preferred_element_type=jnp.float32,
                )
                out_tops.append(new_top)
                out_totals.append(new_total)
                out_accums.append(new_accum)
            return (jnp.stack(out_tops), jnp.stack(out_totals), jnp.stack(out_accums))

        needed = jnp.min(key_pos) <= jnp.max(seg_pos)
        new_parts.append(lax.cond(needed, update, unchanged, carried))
    row_tops, totals, accums = tuple(
        (
            jnp.concatenate([new_part[member] for new_part in new_parts], axis=2)
            for member in range(3)
        )
    )
    map_outputs = accums / totals[..., None]
    mixed_out = map_outputs[0] - lambdas[:, None, None] * map_outputs[1]
    scaled = (
        mixed_out
        * lax.rsqrt(jnp.mean(mixed_out * mixed_out, axis=-1, keepdims=True) + EPS_NORM)
        * head_gain
    )
    attended = scaled.astype(jnp.bfloat16)
    weight_piece = lax.all_gather(out_weight, "sp", axis=1, tiled=True)
    shaped = weight_piece.reshape(heads_here, V, weight_piece.shape[1])
    partial_terms = jnp.einsum("hqv,hvd->qd", attended, shaped, preferred_element_type=jnp.float32)
    summed = lax.psum_scatter(
        partial_terms.astype(jnp.bfloat16), "tp", scatter_dimension=0, tiled=True
    )
    return summed


def solution(mesh):
    in_specs = (
        P(("sp", "tp"), None),
        P("sp", "tp"),
        P("sp", "tp"),
        P("sp", "tp"),
        P("sp", "tp"),
        P("sp", "tp"),
        P("tp", "sp"),
        P("tp"),
        P(),
    )
    out_specs = P(("sp", "tp"), None)
    return jax.shard_map(
        on_device, mesh=mesh, in_specs=in_specs, out_specs=out_specs, check_vma=False
    )
```

profile of v0, /device:TPU:0, one launch (start us, length us, event | category | flops | bytes accessed | tf_op | source)
XLA Modules:
  0.0 554.6 jit_solution(14938328671323246360)
XLA Ops:
  10.5 23.7 %all-gather.11.cloned.1.call-done = bf16[256,4096]{1,0:T(8,128)(2,1)} async-done(((bf16[64,4096]{1,0:T(8,128)(2,1)}), bf16[256,4096]{1,0:T(8,128)(2,1)}) %all-gather.11.cloned.1.call-update) | async-done | bytes 2097168 | tf_op jit(solution)/shard_map/all_gather | solution.py:44
  34.2 74.9 %all-gather.25.cloned.1.call-done = bf16[4096,512]{1,0:T(8,128)(2,1)} async-done(((bf16[512,512]{1,0:T(8,128)(2,1)}), bf16[4096,512]{1,0:T(8,128)(2,1)}) %all-gather.25.cloned.1.call-update) | async-done | bytes 4194320 | tf_op jit(solution)/shard_map/all_gather | solution.py:52
  109.2 4.8 convolution_convert_fusion
  114.3 44.6 %all-gather.19.cloned.1.call-done = bf16[4096,256]{1,0:T(8,128)(2,1)} async-done(((bf16[512,256]{1,0:T(8,128)(2,1)}), bf16[4096,256]{1,0:T(8,128)(2,1)}) %all-gather.19.cloned.1.call-update) | async-done | bytes 2097168 | tf_op jit(solution)/shard_map/all_gather | solution.py:49
  159.0 2.5 fusion.74
  161.5 47.1 %all-gather.21.cloned.1.call-done = bf16[4096,256]{1,0:T(8,128)(2,1)} async-done(((bf16[512,256]{1,0:T(8,128)(2,1)}), bf16[4096,256]{1,0:T(8,128)(2,1)}) %all-gather.21.cloned.1.call-update) | async-done | bytes 2097168 | tf_op jit(solution)/shard_map/all_gather | solution.py:51
  208.6 2.5 fusion.75
  211.1 47.1 %all-gather.13.cloned.1.call-done = bf16[4096,256]{1,0:T(8,128)(2,1)} async-done(((bf16[512,256]{1,0:T(8,128)(2,1)}), bf16[4096,256]{1,0:T(8,128)(2,1)}) %all-gather.13.cloned.1.call-update) | async-done | bytes 2097168 | tf_op jit(solution)/shard_map/all_gather | solution.py:48
  258.2 2.5 fusion.72
  260.7 47.1 %all-gather.15.cloned.1.call-done = bf16[4096,256]{1,0:T(8,128)(2,1)} async-done(((bf16[512,256]{1,0:T(8,128)(2,1)}), bf16[4096,256]{1,0:T(8,128)(2,1)}) %all-gather.15.cloned.1.call-update) | async-done | bytes 2097168 | tf_op jit(solution)/shard_map/all_gather | solution.py:50
  307.8 2.5 fusion.73
  316.8 40.8 %all-gather.27.cloned.1.call-done = bf16[2048,512]{1,0:T(8,128)(2,1)} async-done(((bf16[256,512]{1,0:T(8,128)(2,1)}), bf16[2048,512]{1,0:T(8,128)(2,1)}) %all-gather.27.cloned.1.call-update) | async-done | bytes 2097168 | tf_op jit(solution)/shard_map/all_gather | solution.py:73
  357.6 4.0 reshape.172
  361.6 36.0 %all-gather.23.cloned.1.call-done = bf16[2048,256]{0,1:T(8,128)(2,1)} async-done(((bf16[256,256]{0,1:T(8,128)(2,1)}), bf16[2048,256]{0,1:T(8,128)(2,1)}) %all-gather.23.cloned.1.call-update) | async-done | bytes 1048592 | tf_op jit(solution)/shard_map/all_gather | solution.py:72
  397.6 40.5 %all-gather.17.cloned.1.call-done = bf16[2048,256]{0,1:T(8,128)(2,1)} async-done(((bf16[256,256]{0,1:T(8,128)(2,1)}), bf16[2048,256]{0,1:T(8,128)(2,1)}) %all-gather.17.cloned.1.call-update) | async-done | bytes 1048592 | tf_op jit(solution)/shard_map/all_gather | solution.py:71
  438.1 8.6 %conditional.2 = (f32[2,2,128]{2,1,0:T(2,128)S(1)}, f32[2,2,128,256]{3,2,1,0:T(8,128)}) conditional(s32[]{:T(128)} %convert_element_type.52, () %tuple.21, (s32[2048]{0:T(1024)S(1)}, s32[128]{0:T(128)S(1)}, bf16[256,2,128]{0,2,1:T(8,128)(2,1)S(1)}, bf16[2048,2,128]{0,2,1:T(8,128)(2,1)}, bf16[256,2,128]{0,2,1:T(8,128)(2,1)S(1)}, ...), branch_computations={%region_2.3_spmd, %region_3.8_spmd} | conditional | flops 815136768 | bytes 35283528 | solution.py:129
  439.1 1.9 select_reduce_fusion.1
  441.8 2.1 fusion.5
  446.7 10.4 %conditional.3 = (f32[2,2,128]{2,1,0:T(2,128)S(1)}, f32[2,2,128,256]{3,2,1,0:T(8,128)}) conditional(s32[]{:T(128)} %convert_element_type.57, () %tuple.23, (s32[2048]{0:T(1024)S(1)}, s32[128]{0:T(128)}, bf16[256,2,128]{0,2,1:T(8,128)(2,1)}, bf16[2048,2,128]{0,2,1:T(8,128)(2,1)}, bf16[256,2,128]{0,2,1:T(8,128)(2,1)S(1)}, ...), branch_computations={%region_9.10_spmd, %region_10.15_spmd} | conditional | flops 815136768 | bytes 35283528 | solution.py:129
  449.5 1.9 select_reduce_fusion.3
  452.2 2.1 fusion.31
  458.8 54.9 %all-gather.29.cloned.1.call-done = bf16[512,4096]{1,0:T(8,128)(2,1)} async-done(((bf16[512,512]{1,0:T(8,128)(2,1)}), bf16[512,4096]{1,0:T(8,128)(2,1)}) %all-gather.29.cloned.1.call-update) | async-done | bytes 4194320 | tf_op jit(solution)/shard_map/all_gather | solution.py:144
  513.7 4.8 fusion.52
  518.5 29.5 %reduce-scatter.2.cloned.1.call-done = bf16[64,4096]{1,0:T(8,128)(2,1)} async-done(((bf16[256,4096]{1,0:T(8,128)(2,1)}), bf16[64,4096]{1,0:T(8,128)(2,1)}) %reduce-scatter.2.cloned.1.call-update) | async-done | bytes 524304 | tf_op jit(solution)/shard_map/reduce_scatter | solution.py:147
  (73 shorter events, 20.7 us)
Async XLA Ops:
  6.5 27.7 %all-gather.11.cloned.1.call-start = ((), (), s32[]{:S(2)}) async-start(), calls=%async_computation.1 | async-start | bytes 2621440 | tf_op jit(solution)/shard_map/all_gather | solution.py:44
  7.3 101.9 %all-gather.25.cloned.1.call-start = ((), (), s32[]{:S(2)}) async-start(), calls=%async_computation.8 | async-start | bytes 4718592 | tf_op jit(solution)/shard_map/all_gather | solution.py:52
  8.0 150.9 %all-gather.19.cloned.1.call-start = ((), (), s32[]{:S(2)}) async-start(), calls=%async_computation.5 | async-start | bytes 2359296 | tf_op jit(solution)/shard_map/all_gather | solution.py:49
  8.7 199.9 %all-gather.21.cloned.1.call-start = ((), (), s32[]{:S(2)}) async-start(), calls=%async_computation.6 | async-start | bytes 2359296 | tf_op jit(solution)/shard_map/all_gather | solution.py:51
  9.3 248.9 %all-gather.13.cloned.1.call-start = ((), (), s32[]{:S(2)}) async-start(), calls=%async_computation.2 | async-start | bytes 2359296 | tf_op jit(solution)/shard_map/all_gather | solution.py:48
  9.9 297.9 %all-gather.15.cloned.1.call-start = ((), (), s32[]{:S(2)}) async-start(), calls=%async_computation.3 | async-start | bytes 2359296 | tf_op jit(solution)/shard_map/all_gather | solution.py:50
  10.5 347.1 %all-gather.27.cloned.1.call-start = ((), (), s32[]{:S(2)}) async-start(), calls=%async_computation.9 | async-start | bytes 2359296 | tf_op jit(solution)/shard_map/all_gather | solution.py:73
  34.2 124.7 %copy-start = (bf16[256,4096]{1,0:T(8,128)(2,1)S(1)}, bf16[256,4096]{1,0:T(8,128)(2,1)}, u32[]{:S(2)}) copy-start(bf16[256,4096]{1,0:T(8,128)(2,1)} %all-gather.11.cloned.1.call-done) | copy-start | bytes 6291460
  114.0 283.7 %all-gather.23.cloned.1.call-start = ((), (), s32[]{:S(2)}) async-start(), calls=%async_computation.7 | async-start | bytes 1179648 | tf_op jit(solution)/shard_map/all_gather | solution.py:72
  311.2 126.9 %all-gather.17.cloned.1.call-start = ((), (), s32[]{:S(2)}) async-start(), calls=%async_computation.4 | async-start | bytes 1179648 | tf_op jit(solution)/shard_map/all_gather | solution.py:71
  312.0 201.7 %all-gather.29.cloned.1.call-start = ((), (), s32[]{:S(2)}) async-start(), calls=%async_computation.10 | async-start | bytes 4718592 | tf_op jit(solution)/shard_map/all_gather | solution.py:144
  312.5 235.5 %reduce-scatter.2.cloned.1.call-start = ((), (), s32[]{:S(2)}) async-start(), calls=%async_computation.11 | async-start | bytes 2621440 | tf_op jit(solution)/shard_map/reduce_scatter | solution.py:147
  316.8 121.3 %copy-start.5 = (bf16[256,2,128]{0,2,1:T(8,128)(2,1)}, bf16[256,2,128]{0,2,1:T(8,128)(2,1)S(1)}, u32[]{:S(2)}) copy-start(bf16[256,2,128]{0,2,1:T(8,128)(2,1)S(1)} %pad_maximum_fusion.4) | copy-start | bytes 393220
  438.1 3.7 copy-start.1
  441.8 2.1 copy-start.3
  446.9 5.3 copy-start.2
  452.2 2.1 copy-start.4
  457.1 1.5 copy-start.6
  457.1 56.6 %copy-start.7 = (f32[256]{0:T(256)S(1)}, f32[256]{0:T(256)}, u32[]{:S(2)}) copy-start(f32[256]{0:T(256)} %param.21) | copy-start | bytes 3076
Sparse Core Ops, SparseCore 0:
  8.9 25.2 all-gather.10
  36.3 72.7 all-gather.24
  111.3 47.6 all-gather.18
  160.9 47.6 all-gather.20
  210.6 47.5 all-gather.12
  260.2 47.6 all-gather.14
  310.0 47.6 all-gather.26
  359.7 37.9 all-gather.22
  399.7 38.3 all-gather.16
  440.0 73.6 all-gather.28
  518.7 29.3 reduce-scatter.1
where the time goes:
time: 555 us
  waiting for transfers between devices  490 us (88%)
  matrix products  30.4 us (5%)
  between operations  15.7 us (3%)
  other arithmetic  9.28 us (2%)
  local copies, waits for them, and re-layouts  7.99 us (1%)
    all_gather x1, waiting for transfers between devices, on_device(): lax.all_gather(value_weight, 'sp', axis=0, tiled=True)  74.9 us
    all_gather x1, waiting for transfers between devices, on_device(): weight_piece = lax.all_gather(out_weight, 'sp', axis=1, tiled=True)  54.9 us
    all_gather x1, waiting for transfers between devices, on_device(): lax.all_gather(key_two, 'sp', axis=0, tiled=True)  47.1 us
    all_gather x1, waiting for transfers between devices, on_device(): lax.all_gather(key_one, 'sp', axis=0, tiled=True)  47.1 us
    all_gather x1, waiting for transfers between devices, on_device(): lax.all_gather(query_one, 'sp', axis=0, tiled=True)  47.1 us
    all_gather x1, waiting for transfers between devices, on_device(): lax.all_gather(query_two, 'sp', axis=0, tiled=True)  44.6 us
    all_gather x1, waiting for transfers between devices, on_device(): lax.all_gather(values, 'sp', axis=0, tiled=True)  40.8 us
    all_gather x1, waiting for transfers between devices, on_device(): lax.all_gather(k_one, 'sp', axis=0, tiled=True)  40.5 us
  transfers between devices with their start and end apart: 11, of which 11 were waited for; matrix products, arithmetic and copies ran while one was open for 8% of the time, Pallas kernels for 0%

commit v1 on v0

--- a/solution.py
+++ b/solution.py
@@ -7,6 +7,28 @@
 V = 256
 ROPE_BASE = 500000.0
 EPS_NORM = 0.02
+
+
+def bring_the_cube(piece_in, row_dim):
+    local_now = list(piece_in.shape[1:])
+    local_now[row_dim] *= piece_in.shape[0]
+    return jnp.moveaxis(piece_in, 0, row_dim).reshape(local_now)
+
+
+def wrap_the_map(inp, a_name):
+    state_now = lax.axis_size(a_name)
+    latest = lax.axis_index(a_name)
+    part_now, view_out = (state_now, latest)
+    carry_out, heard = (inp[None], 1)
+    while heard < part_now:
+        a_now = tuple(((nth, nth ^ heard) for nth in range(part_now)))
+        reached = lax.ppermute(carry_out, axis_name=a_name, perm=a_now)
+        fresh = view_out & heard == 0
+        item_now = jnp.where(fresh, carry_out, reached)
+        y_new = jnp.where(fresh, reached, carry_out)
+        carry_out = jnp.concatenate([item_now, y_new])
+        heard *= 2
+    return carry_out
 
 
 def rotate(values, positions):
@@ -35,6 +57,10 @@
 def on_device(
     tokens, query_one, query_two, key_one, key_two, value_weight, out_weight, lambdas, head_gain
 ):
+
+    def recover_rows_over_axis(x_in, block_in, join_dim):
+        return bring_the_cube(wrap_the_map(block_in, x_in), join_dim)
+
     tp_count = lax.axis_size("tp")
     sp_index = lax.axis_index("sp")
     own_rows = tokens.shape[0]
@@ -47,7 +73,7 @@
     pieces = (
         lax.all_gather(query_one, "sp", axis=0, tiled=True),
         lax.all_gather(query_two, "sp", axis=0, tiled=True),
-        lax.all_gather(key_one, "sp", axis=0, tiled=True),
+        recover_rows_over_axis("sp", key_one, 0),
         lax.all_gather(key_two, "sp", axis=0, tiled=True),
         lax.all_gather(value_weight, "sp", axis=0, tiled=True),
     )

time: 555 us -> 546 us (0.984)
  waiting for transfers between devices: 490 us -> 472 us
  starting transfers between devices: 0.39 us -> 7.15 us
    ppermute x0 -> x3, waiting for transfers between devices: none -> 60 us  [wrap_the_map(): reached = lax.ppermute(carry_out, axis_name=a_name, perm=a_now)]
    all_gather x1 -> x0, waiting for transfers between devices: 47.1 us -> none  [on_device(): lax.all_gather(key_one, 'sp', axis=0, tiled=True)]
    all_gather x1, waiting for transfers between devices: 44.6 us -> 25.2 us  [on_device(): lax.all_gather(query_two, 'sp', axis=0, tiled=True)]
    all_gather x1, waiting for transfers between devices: 23.7 us -> 11.7 us  [on_device(): gathered = lax.all_gather(tokens, 'tp', axis=0, tiled=True)]
    ppermute x0 -> x3, starting transfers between devices: none -> 6.79 us  [wrap_the_map(): reached = lax.ppermute(carry_out, axis_name=a_name, perm=a_now)]
  transfers between devices with their start and end apart: 11 -> 13, of which waited for: 11 -> 12; matrix products, arithmetic and copies ran while one was open for 8% -> 8% of each run, Pallas kernels for 0% -> 0%
where the time goes in v1:
time: 546 us
  waiting for transfers between devices  472 us (86%)
  matrix products  28.7 us (5%)
  between operations  16.3 us (3%)
  other arithmetic  11.8 us (2%)
  local copies, waits for them, and re-layouts  9.4 us (2%)
  starting transfers between devices  7.15 us (1%)
    all_gather x1, waiting for transfers between devices, on_device(): lax.all_gather(value_weight, 'sp', axis=0, tiled=True)  75 us
    ppermute x3, waiting for transfers between devices, wrap_the_map(): reached = lax.ppermute(carry_out, axis_name=a_name, perm=a_now)  60 us
    all_gather x1, waiting for transfers between devices, on_device(): weight_piece = lax.all_gather(out_weight, 'sp', axis=1, tiled=True)  55.8 us
    all_gather x1, waiting for transfers between devices, on_device(): lax.all_gather(key_two, 'sp', axis=0, tiled=True)  47.1 us
    all_gather x1, waiting for transfers between devices, on_device(): lax.all_gather(query_one, 'sp', axis=0, tiled=True)  47.1 us
    all_gather x1, waiting for transfers between devices, on_device(): lax.all_gather(k_one, 'sp', axis=0, tiled=True)  40.5 us
    all_gather x1, waiting for transfers between devices, on_device(): lax.all_gather(values, 'sp', axis=0, tiled=True)  40.2 us
    all_gather x1, waiting for transfers between devices, on_device(): lax.all_gather(k_two, 'sp', axis=0, tiled=True)  36 us
  transfers between devices with their start and end apart: 13, of which 12 were waited for; matrix products, arithmetic and copies ran while one was open for 8% of the time, Pallas kernels for 0%

profile of v1, /device:TPU:0, one launch (start us, length us, event | category | flops | bytes accessed | tf_op | source)
XLA Modules:
  0.0 545.6 jit_solution(963950363977366892)
XLA Ops:
  10.0 3.1 collective-permute-start
  13.0 6.5 %collective-permute-done = bf16[1,512,256]{2,1,0:T(8,128)(2,1)S(1)} collective-permute-done((bf16[1,512,256]{2,1,0:T(8,128)(2,1)}, bf16[1,512,256]{2,1,0:T(8,128)(2,1)S(1)}, u32[]{:S(2)}, u32[]{:S(2)}) %collective-permute-start) | collective-permute-done | bytes 262176 | tf_op jit(solution)/shard_map/ppermute | solution.py:25
  22.5 11.7 %all-gather.10.cloned.1.call-done = bf16[256,4096]{1,0:T(8,128)(2,1)} async-done(((bf16[64,4096]{1,0:T(8,128)(2,1)}), bf16[256,4096]{1,0:T(8,128)(2,1)}) %all-gather.10.cloned.1.call-update) | async-done | bytes 2097168 | tf_op jit(solution)/shard_map/all_gather | solution.py:70
  34.2 75.0 %all-gather.22.cloned.1.call-done = bf16[4096,512]{1,0:T(8,128)(2,1)} async-done(((bf16[512,512]{1,0:T(8,128)(2,1)}), bf16[4096,512]{1,0:T(8,128)(2,1)}) %all-gather.22.cloned.1.call-update) | async-done | bytes 4194320 | tf_op jit(solution)/shard_map/all_gather | solution.py:78
  109.2 4.8 convolution_convert_fusion
  117.4 53.5 %collective-permute-done.2 = bf16[4,512,256]{2,1,0:T(8,128)(2,1)S(1)} collective-permute-done((bf16[4,512,256]{2,1,0:T(8,128)(2,1)}, bf16[4,512,256]{2,1,0:T(8,128)(2,1)S(1)}, u32[]{:S(2)}, u32[]{:S(2)}) %collective-permute-start.2) | collective-permute-done | bytes 1048608 | tf_op jit(solution)/shard_map/ppermute | solution.py:25
  173.4 25.2 %all-gather.16.cloned.1.call-done = bf16[4096,256]{1,0:T(8,128)(2,1)} async-done(((bf16[512,256]{1,0:T(8,128)(2,1)}), bf16[4096,256]{1,0:T(8,128)(2,1)}) %all-gather.16.cloned.1.call-update) | async-done | bytes 2097168 | tf_op jit(solution)/shard_map/all_gather | solution.py:75
  198.6 2.5 fusion.74
  201.1 47.1 %all-gather.18.cloned.1.call-done = bf16[4096,256]{1,0:T(8,128)(2,1)} async-done(((bf16[512,256]{1,0:T(8,128)(2,1)}), bf16[4096,256]{1,0:T(8,128)(2,1)}) %all-gather.18.cloned.1.call-update) | async-done | bytes 2097168 | tf_op jit(solution)/shard_map/all_gather | solution.py:77
  248.2 2.5 fusion.75
  250.8 47.1 %all-gather.12.cloned.1.call-done = bf16[4096,256]{1,0:T(8,128)(2,1)} async-done(((bf16[512,256]{1,0:T(8,128)(2,1)}), bf16[4096,256]{1,0:T(8,128)(2,1)}) %all-gather.12.cloned.1.call-update) | async-done | bytes 2097168 | tf_op jit(solution)/shard_map/all_gather | solution.py:74
  297.8 2.5 fusion.72
  307.3 40.2 %all-gather.24.cloned.1.call-done = bf16[2048,512]{1,0:T(8,128)(2,1)} async-done(((bf16[256,512]{1,0:T(8,128)(2,1)}), bf16[2048,512]{1,0:T(8,128)(2,1)}) %all-gather.24.cloned.1.call-update) | async-done | bytes 2097168 | tf_op jit(solution)/shard_map/all_gather | solution.py:99
  347.5 4.0 reshape.176
  351.5 36.0 %all-gather.20.cloned.1.call-done = bf16[2048,256]{0,1:T(8,128)(2,1)} async-done(((bf16[256,256]{0,1:T(8,128)(2,1)}), bf16[2048,256]{0,1:T(8,128)(2,1)}) %all-gather.20.cloned.1.call-update) | async-done | bytes 1048592 | tf_op jit(solution)/shard_map/all_gather | solution.py:98
  387.5 40.5 %all-gather.14.cloned.1.call-done = bf16[2048,256]{0,1:T(8,128)(2,1)} async-done(((bf16[256,256]{0,1:T(8,128)(2,1)}), bf16[2048,256]{0,1:T(8,128)(2,1)}) %all-gather.14.cloned.1.call-update) | async-done | bytes 1048592 | tf_op jit(solution)/shard_map/all_gather | solution.py:97
  428.0 8.6 %conditional.2 = (f32[2,2,128]{2,1,0:T(2,128)S(1)}, f32[2,2,128,256]{3,2,1,0:T(8,128)}) conditional(s32[]{:T(128)} %convert_element_type.52, () %tuple.21, (s32[2048]{0:T(1024)S(1)}, s32[128]{0:T(128)S(1)}, bf16[256,2,128]{0,2,1:T(8,128)(2,1)S(1)}, bf16[2048,2,128]{0,2,1:T(8,128)(2,1)}, bf16[256,2,128]{0,2,1:T(8,128)(2,1)S(1)}, ...), branch_computations={%region_2.3_spmd, %region_3.8_spmd} | conditional | flops 815136768 | bytes 35283528 | solution.py:155
  429.0 1.9 select_reduce_fusion.1
  431.7 2.1 fusion.5
  436.5 10.4 %conditional.3 = (f32[2,2,128]{2,1,0:T(2,128)S(1)}, f32[2,2,128,256]{3,2,1,0:T(8,128)}) conditional(s32[]{:T(128)} %convert_element_type.57, () %tuple.23, (s32[2048]{0:T(1024)S(1)}, s32[128]{0:T(128)}, bf16[256,2,128]{0,2,1:T(8,128)(2,1)}, bf16[2048,2,128]{0,2,1:T(8,128)(2,1)}, bf16[256,2,128]{0,2,1:T(8,128)(2,1)S(1)}, ...), branch_computations={%region_9.10_spmd, %region_10.15_spmd} | conditional | flops 815136768 | bytes 35283528 | solution.py:155
  442.0 2.1 fusion.31
  448.6 55.8 %all-gather.26.cloned.1.call-done = bf16[512,4096]{1,0:T(8,128)(2,1)} async-done(((bf16[512,512]{1,0:T(8,128)(2,1)}), bf16[512,4096]{1,0:T(8,128)(2,1)}) %all-gather.26.cloned.1.call-update) | async-done | bytes 4194320 | tf_op jit(solution)/shard_map/all_gather | solution.py:170
  504.5 4.8 fusion.52
  509.3 29.5 %reduce-scatter.2.cloned.1.call-done = bf16[64,4096]{1,0:T(8,128)(2,1)} async-done(((bf16[256,4096]{1,0:T(8,128)(2,1)}), bf16[64,4096]{1,0:T(8,128)(2,1)}) %reduce-scatter.2.cloned.1.call-update) | async-done | bytes 524304 | tf_op jit(solution)/shard_map/reduce_scatter | solution.py:173
  (82 shorter events, 30.7 us)
Async XLA Ops:
  6.5 27.7 %all-gather.10.cloned.1.call-start = ((), (), s32[]{:S(2)}) async-start(), calls=%async_computation.1 | async-start | bytes 2621440 | tf_op jit(solution)/shard_map/all_gather | solution.py:70
  7.3 101.9 %all-gather.22.cloned.1.call-start = ((), (), s32[]{:S(2)}) async-start(), calls=%async_computation.7 | async-start | bytes 4718592 | tf_op jit(solution)/shard_map/all_gather | solution.py:78
  8.0 190.6 %all-gather.16.cloned.1.call-start = ((), (), s32[]{:S(2)}) async-start(), calls=%async_computation.4 | async-start | bytes 2359296 | tf_op jit(solution)/shard_map/all_gather | solution.py:75
  8.7 239.5 %all-gather.18.cloned.1.call-start = ((), (), s32[]{:S(2)}) async-start(), calls=%async_computation.5 | async-start | bytes 2359296 | tf_op jit(solution)/shard_map/all_gather | solution.py:77
  9.3 288.5 %all-gather.12.cloned.1.call-start = ((), (), s32[]{:S(2)}) async-start(), calls=%async_computation.2 | async-start | bytes 2359296 | tf_op jit(solution)/shard_map/all_gather | solution.py:74
  9.9 337.6 %all-gather.24.cloned.1.call-start = ((), (), s32[]{:S(2)}) async-start(), calls=%async_computation.8 | async-start | bytes 2359296 | tf_op jit(solution)/shard_map/all_gather | solution.py:99
  10.0 9.6 %collective-permute-start = (bf16[1,512,256]{2,1,0:T(8,128)(2,1)}, bf16[1,512,256]{2,1,0:T(8,128)(2,1)S(1)}, u32[]{:S(2)}, u32[]{:S(2)}) collective-permute-start(bf16[1,512,256]{2,1,0:T(8,128)(2,1)} %bitcast.70), channel_id=1, source_target_pairs={{0,4},{4,0},{8,12},{12,8},{16,20},{20,16},{24,28},{28,24},{1,5},{5... | collective-permute-start | bytes 786440 | tf_op jit(solution)/shard_map/ppermute | solution.py:25
  20.6 93.4 %collective-permute-start.1 = (bf16[2,512,256]{2,1,0:T(8,128)(2,1)S(1)}, bf16[2,512,256]{2,1,0:T(8,128)(2,1)S(1)}, u32[]{:S(2)}, u32[]{:S(2)}) collective-permute-start(bf16[2,512,256]{2,1,0:T(8,128)(2,1)S(1)} %pad_maximum_fusion.6), channel_id=1, source_target_pairs={{0,8},{4,12},{8,0},{12,4},{16,24},{20,28},{24,16},{28,20},{1,9},{5... | collective-permute-start | bytes 1572872 | tf_op jit(solution)/shard_map/ppermute | solution.py:25
  114.0 273.5 %all-gather.20.cloned.1.call-start = ((), (), s32[]{:S(2)}) async-start(), calls=%async_computation.6 | async-start | bytes 1179648 | tf_op jit(solution)/shard_map/all_gather | solution.py:98
  115.2 55.7 %collective-permute-start.2 = (bf16[4,512,256]{2,1,0:T(8,128)(2,1)}, bf16[4,512,256]{2,1,0:T(8,128)(2,1)S(1)}, u32[]{:S(2)}, u32[]{:S(2)}) collective-permute-start(bf16[4,512,256]{2,1,0:T(8,128)(2,1)} %pad_maximum_fusion.5), channel_id=1, source_target_pairs={{0,16},{4,20},{8,24},{12,28},{16,0},{20,4},{24,8},{28,12},{1,17},{... | collective-permute-start | bytes 3145736 | tf_op jit(solution)/shard_map/ppermute | solution.py:25
  171.0 1.6 copy-start
  301.2 126.7 %all-gather.14.cloned.1.call-start = ((), (), s32[]{:S(2)}) async-start(), calls=%async_computation.3 | async-start | bytes 1179648 | tf_op jit(solution)/shard_map/all_gather | solution.py:97
  302.0 202.5 %all-gather.26.cloned.1.call-start = ((), (), s32[]{:S(2)}) async-start(), calls=%async_computation.9 | async-start | bytes 4718592 | tf_op jit(solution)/shard_map/all_gather | solution.py:170
  302.7 236.1 %reduce-scatter.2.cloned.1.call-start = ((), (), s32[]{:S(2)}) async-start(), calls=%async_computation.10 | async-start | bytes 2621440 | tf_op jit(solution)/shard_map/reduce_scatter | solution.py:173
  307.3 120.7 %copy-start.5 = (bf16[256,2,128]{0,2,1:T(8,128)(2,1)}, bf16[256,2,128]{0,2,1:T(8,128)(2,1)S(1)}, u32[]{:S(2)}) copy-start(bf16[256,2,128]{0,2,1:T(8,128)(2,1)S(1)} %pad_maximum_fusion.7) | copy-start | bytes 393220
  428.0 3.7 copy-start.1
  431.7 2.1 copy-start.3
  436.7 5.3 copy-start.2
  442.0 2.1 copy-start.4
  446.9 1.5 copy-start.6
  446.9 57.5 %copy-start.7 = (f32[256]{0:T(256)S(1)}, f32[256]{0:T(256)}, u32[]{:S(2)}) copy-start(f32[256]{0:T(256)} %param.21) | copy-start | bytes 3076
Sparse Core Ops, SparseCore 0:
  8.9 25.2 all-gather.9
  36.3 72.7 all-gather.21
  111.3 87.2 all-gather.15
  200.6 47.6 all-gather.17
  250.2 47.5 all-gather.11
  299.8 47.6 all-gather.23
  349.5 37.9 all-gather.19
  389.5 38.3 all-gather.13
  430.0 74.3 all-gather.25
  509.4 29.3 reduce-scatter.1
